TPU v7x, 32 devices: a whole 2x2x4 slice. The times are simulated.
32 devices in a mesh: sp: 8 (over z, y), tp: 4 (over x, core).
Axes of the slice: x: 2, y: 2, z: 4, core: 2. Of those that a mesh axis runs over, the one named last changes fastest.
Arguments:
- tokens: bfloat16 [2048, 2048], P('sp', 'tp'), may hold values from -19 to 250
- in_gain: bfloat16 [2048], replicated, may hold values from 0.099609375 to 1.8984375
- w_glu_value: bfloat16 [2048, 512], P(None, 'tp'), may hold values from -0.125 to 0.125
- w_glu_gate: bfloat16 [2048, 512], P(None, 'tp'), may hold values from -0.125 to 0.125
- w_query: bfloat16 [2048, 1024], P(None, 'tp'), may hold values from -1 to 1
- w_key: bfloat16 [2048, 512], P(None, 'tp'), may hold values from -1 to 1
- w_value: bfloat16 [2048, 512], P(None, 'tp'), may hold values from -0.125 to 0.125
- w_gate_conv: bfloat16 [2048, 512], P(None, 'tp'), may hold values from -0.125 to 0.125
- w_gate_attn: bfloat16 [2048, 1024], P(None, 'tp'), may hold values from -0.125 to 0.125
- conv_weight: bfloat16 [31, 512], P(None, 'tp'), may hold values from -4.6 to 4.6
- conv_gain: float32 [512], P('tp'), may hold values from 0.1 to 1.9
- lam: float32 [8], P('tp'), may hold values from 0.3 to 0.8
- head_gain: float32 [128], replicated, may hold values from 0.1 to 1.9
- out_conv: bfloat16 [512, 2048], P('tp'), may hold values from -0.15625 to 0.15625
- out_attn: bfloat16 [1024, 2048], P('tp'), may hold values from -0.15625 to 0.15625
Outputs:
- mixed: bfloat16 [2048, 2048], P(('sp', 'tp'))
All inputs are finite; a program needn't handle non-finite values.
Results may differ from a plain program's by a relative error of at most 0.017.
The roundings to bfloat16 on the way count: a program that leaves them out, or rounds other values in their place, can miss the bound.
Values may be sent and summed in bfloat16 or wider, within the bound.
A program may use at most 128 MiB of HBM per device.

v0:
```python
import math
import jax
import jax.numpy as jnp
from jax import lax
from jax.sharding import PartitionSpec as P

D = 2048
CONV = 512
QK = 64
VDIM = 128
WIDTH = 31
EPSILON = 1e-06
NEG_BIG = -1e30
HEAD_SCALE = 0.8


def shifted(x, axis, by):
    count = lax.axis_size(axis)
    pairs = [(i, i + by) for i in range(count) if 0 <= i + by < count]
    return lax.ppermute(x, axis, pairs)


def local(
    tokens,
    in_gain,
    w_glu_value,
    w_glu_gate,
    w_query,
    w_key,
    w_value,
    w_gate_conv,
    w_gate_attn,
    conv_weight,
    conv_gain,
    lam,
    head_gain,
    out_conv,
    out_attn,
):
    tok_rows = tokens.shape[0]
    weights = (w_glu_value, w_glu_gate, w_query, w_key, w_value, w_gate_conv, w_gate_attn)
    widened = lax.all_gather(tokens, "tp", axis=1, tiled=True).astype(jnp.float32)
    gain_part = in_gain.astype(jnp.float32)
    scaled = (widened * gain_part[None, :]).astype(jnp.bfloat16)
    updated = tuple(
        (jnp.dot(scaled, weight, preferred_element_type=jnp.float32) for weight in weights)
    )
    squares = jnp.sum(widened * widened, axis=1)
    inv_rms = lax.rsqrt(squares / D + EPSILON)[:, None]
    glu_value, glu_gate, query, key, value, gate_conv, gate_attn = [
        (total * inv_rms).astype(jnp.bfloat16) for total in updated
    ]
    glued = (glu_value.astype(jnp.float32) * jax.nn.sigmoid(glu_gate.astype(jnp.float32))).astype(
        jnp.bfloat16
    )
    tail_rows = WIDTH - 1
    last_rows = glued[tok_rows - tail_rows :]
    conv_local = glued.shape[1]
    kv_local = key.shape[1] // (2 * QK)
    heads_local = lam.shape[0]
    group = heads_local // kv_local
    my_index = lax.axis_index("sp")
    my_start = my_index * tok_rows
    scale_factor = 1.0 / math.sqrt(QK)
    query_groups = [
        (
            query.reshape(tok_rows, kv_local, group, 2, QK),
            my_start + jnp.arange(tok_rows, dtype=jnp.int32),
        )
    ]
    start_attn = tuple(
        (
            (
                jnp.full((kv_local, group, 2, rows_of.shape[0]), NEG_BIG, jnp.float32),
                jnp.zeros((kv_local, group, 2, rows_of.shape[0]), jnp.float32),
                jnp.zeros((kv_local, group, 2, rows_of.shape[0], VDIM), jnp.float32),
            )
            for rows_of, unused_pos in query_groups
        )
    )
    key_piece = lax.all_gather(key, "sp", axis=0, tiled=True)
    value_piece = lax.all_gather(value, "sp", axis=0, tiled=True)
    shards = key_piece.shape[0] // tok_rows
    stacked_keys = key_piece.reshape(shards, tok_rows, kv_local, 2, QK)
    stacked_values = value_piece.reshape(shards, tok_rows, kv_local, VDIM)
    firsts = tok_rows * jnp.arange(shards, dtype=jnp.int32)

    def visit(states, inputs):
        key_shard, value_shard, first = inputs
        key_pos = first + jnp.arange(tok_rows, dtype=jnp.int32)
        updated_states = []
        for (query_rows, query_pos), current_state in zip(query_groups, states):

            def update(current, query_rows=query_rows, query_pos=query_pos):
                maxima, totals, summed = current
                scores = (
                    jnp.einsum(
                        "qagcd,kacd->agcqk",
                        query_rows,
                        key_shard,
                        preferred_element_type=jnp.float32,
                    )
                    * scale_factor
                )
                allowed = key_pos[None, :] <= query_pos[:, None]
                scores = jnp.where(allowed, scores, NEG_BIG)
                new_max = jnp.maximum(maxima, jnp.max(scores, axis=4))
                factor = jnp.exp(maxima - new_max)
                expd = jnp.exp(scores - new_max[..., None])
                totals = totals * factor + jnp.sum(expd, axis=4)
                summed = summed * factor[..., None] + jnp.einsum(
                    "agcqk,kav->agcqv",
                    expd.astype(jnp.bfloat16),
                    value_shard,
                    preferred_element_type=jnp.float32,
                )
                return (new_max, totals, summed)

            def keep(current):
                return current

            query_last = query_pos[0] + query_pos.shape[0] - 1
            updated_states.append(lax.cond(first <= query_last, update, keep, current_state))
        return (tuple(updated_states), None)

    result, unused = lax.scan(visit, start_attn, (stacked_keys, stacked_values, firsts))
    states = result
    maxima, totals, summed = states[0]
    output = (
        summed[:, :, 0] / totals[:, :, 0][..., None]
        - lam.reshape(kv_local, group)[:, :, None, None]
        * summed[:, :, 1]
        / totals[:, :, 1][..., None]
    )
    normed = output * lax.rsqrt(jnp.mean(output * output, axis=3, keepdims=True) + EPSILON)
    normed = normed * head_gain[None, None, None, :] * HEAD_SCALE
    laid = jnp.transpose(normed, (2, 0, 1, 3)).reshape(normed.shape[2], heads_local * VDIM)
    y_attn = (laid * jax.nn.silu(gate_attn.astype(jnp.float32))).astype(jnp.bfloat16)
    previous = shifted(last_rows, "sp", 1)
    padded = jnp.concatenate([previous, glued], axis=0).astype(jnp.float32)
    taps = conv_weight.astype(jnp.float32)
    conv = jnp.zeros((tok_rows, conv_local), jnp.float32)
    for offset in range(WIDTH):
        conv = conv + padded[offset : offset + tok_rows] * taps[offset][None, :]
    total_sq = lax.psum(jnp.sum(conv * conv, axis=1), "tp")
    normed = conv * lax.rsqrt(total_sq / CONV + EPSILON)[:, None] * conv_gain[None, :]
    y_conv = (jax.nn.silu(normed) * jax.nn.silu(gate_conv.astype(jnp.float32))).astype(jnp.bfloat16)
    return lax.psum_scatter(
        (
            jnp.dot(y_conv, out_conv, preferred_element_type=jnp.float32)
            + jnp.dot(y_attn, out_attn, preferred_element_type=jnp.float32)
        ).astype(jnp.bfloat16),
        "tp",
        scatter_dimension=0,
        tiled=True,
    )


def solution(mesh):
    in_specs = (
        P("sp", "tp"),
        P(),
        P(None, "tp"),
        P(None, "tp"),
        P(None, "tp"),
        P(None, "tp"),
        P(None, "tp"),
        P(None, "tp"),
        P(None, "tp"),
        P(None, "tp"),
        P("tp"),
        P("tp"),
        P(),
        P("tp", None),
        P("tp", None),
    )
    out_specs = P(("sp", "tp"), None)
    return jax.shard_map(local, mesh=mesh, in_specs=in_specs, out_specs=out_specs, check_vma=False)
```

profile of v0, /device:TPU:0, one launch (start us, length us, event | category | flops | bytes accessed | tf_op | source)
XLA Modules:
  0.0 186.6 jit_solution(6918326451705439415)
XLA Ops:
  6.5 0.7 all-gather.2.cloned.1.call-update
  7.3 0.7 convert_element_type.71
  8.5 0.7 convert_element_type.79
  9.8 18.6 %all-gather.2.cloned.1.call-done = bf16[256,2048]{1,0:T(8,128)(2,1)} async-done(((bf16[256,512]{1,0:T(8,128)(2,1)}), bf16[256,2048]{1,0:T(8,128)(2,1)}) %all-gather.2.cloned.1.call-update) | async-done | bytes 1048592 | tf_op jit(solution)/shard_map/all_gather | solution.py:42
  28.3 1.5 fusion.19
  29.9 1.8 fusion.35
  31.7 33.5 %all_gather.10 = bf16[2048,128]{1,0:T(8,128)(2,1)} all-gather(bf16[256,128]{1,0:T(8,128)(2,1)S(1)} %fusion.35), channel_id=1, replica_groups=mesh['sp'=8,'tp'=4] {'sp'}, dimensions={0}, use_global_device_ids=true | all-gather | bytes 589824 | tf_op jit(solution)/shard_map/all_gather | solution.py:81
  65.2 2.4 %reshape.159 = bf16[8,256,1,2,64]{4,3,1,0,2:T(2,128)(2,1)S(1)} reshape(bf16[2048,128]{1,0:T(8,128)(2,1)} %all_gather.10) | data formatting | bytes 1048576 | tf_op jit(solution)/shard_map/reshape | solution.py:84
  67.6 1.8 copy.27
  69.4 1.6 fusion.36
  70.9 31.3 %all_gather.11 = bf16[2048,128]{1,0:T(8,128)(2,1)S(1)} all-gather(bf16[256,128]{1,0:T(8,128)(2,1)S(1)} %fusion.36), channel_id=1, replica_groups=mesh['sp'=8,'tp'=4] {'sp'}, dimensions={0}, use_global_device_ids=true | all-gather | bytes 589824 | tf_op jit(solution)/shard_map/all_gather | solution.py:82
  102.9 13.8 %while.17 = (s32[]{:T(128)}, f32[1,2,2,256]{3,1,2,0:T(2,128)S(1)}, f32[1,2,2,256]{3,1,2,0:T(2,128)S(1)}, f32[1,2,2,256,128]{4,3,2,1,0:T(8,128)S(1)}, s32[8]{0:T(...) while((s32[]{:T(128)}, f32[1,2,2,256]{3,1,2,0:T(2,128)S(1)}, ...), condition=%wide.region_8.9_spmd.clone, body=%wide.region_3.8_spmd.clone.sunk | while | flops 102567424 | bytes 4665123 | solution.py:126
  102.9 0.7 dynamic_slice.38
  104.3 2.8 %conditional.3 = ((f32[1,2,2,256]{3,1,2,0:T(2,128)S(1)}, f32[1,2,2,256]{3,1,2,0:T(2,128)S(1)}, f32[1,2,2,256,128]{4,3,2,1,0:T(8,128)S(1)})) conditional(s32[]{:T(128)} %convert_element_type.190, (f32[1,2,2,256]{3,1,2,0:T(2,128)S(1)}, f32[1,2,2,256]{3,1,2,0:T(2,128)S(1)}, f32[1,2,2,256,128]{4,3,2,1,0:T(8,128)S(1)}) %tuple.82, (s32[]{:T(128)}, ...), branch_computations={%region_4.4_spmd, %region_5.7_spmd} | conditional | flops 102567424 | bytes 4663852 | solution.py:123
  104.3 0.7 broadcast_add_fusion
  105.1 1.2 fusion.99
  108.5 0.7 dynamic_slice.38
  117.4 1.6 fusion.32
  119.4 6.5 %collective-permute-start = (bf16[30,128]{1,0:T(8,128)(2,1)S(1)}, bf16[30,128]{1,0:T(8,128)(2,1)S(1)}, u32[]{:S(2)}, u32[]{:S(2)}) collective-permute-start(bf16[30,128]{1,0:T(8,128)(2,1)S(1)} %slice.274), channel_id=1, source_target_pairs={{0,4},{4,8},{8,12},{12,16},{16,20},{20,24},{24,28},{1,5},{5,9},{9,... | collective-permute-start | bytes 23048 | tf_op jit(solution)/shard_map/ppermute | solution.py:20
  126.5 0.7 collective-permute-done
  127.9 5.8 %psum.7 = f32[256]{0:T(256)S(1)} all-reduce(f32[256]{0:T(256)S(1)} %get-tuple-element.287), channel_id=1, replica_groups=mesh['sp'=8,'tp'=4] {'tp'}, use_global_device_ids=true, to_apply=%region_2.3 | all-reduce | flops 256 | bytes 2048 | tf_op jit(solution)/shard_map/psum | solution.py:145
  133.7 2.3 %fusion.83 = f32[256,2048]{1,0:T(8,128)S(1)} fusion(bf16[128,2048]{1,0:T(8,128)(2,1)} %param.32, bf16[2048,128]{1,0:T(8,128)(2,1)} %param.26, bf16[256,2048]{1,0:T(8,128)(2,1)} %all-gather.2.cloned.1.call-done, f32[2048]{0:T(1024)S(1)} %convert_element_type.71, f32[256,128]{1,0:T(8,128)S(1)} %get-tuple-element.288, f32[128]{0:T(128)S(1)} %copy-done.3, ...), kind=kOutput, calls=%fused_computation.126 | convolution fusion | flops 270499840 | bytes 4336128 | tf_op jit(solution)/shard_map/dot_general | solution.py:150
  136.0 1.4 fusion.17
  137.4 42.3 %reduce-scatter.2.cloned.1.call-done = bf16[64,2048]{1,0:T(8,128)(2,1)} async-done(((bf16[256,2048]{1,0:T(8,128)(2,1)}), bf16[64,2048]{1,0:T(8,128)(2,1)}) %reduce-scatter.2.cloned.1.call-update) | async-done | bytes 262160 | tf_op jit(solution)/shard_map/reduce_scatter | solution.py:148
  (69 shorter events, 8.3 us)
Async XLA Ops:
  6.5 129.4 %copy-start = (bf16[256,2048]{1,0:T(8,128)(2,1)S(1)}, bf16[256,2048]{1,0:T(8,128)(2,1)}, u32[]{:S(2)}) copy-start(bf16[256,2048]{1,0:T(8,128)(2,1)} %param.33) | copy-start | bytes 3145732
  6.5 21.8 %all-gather.2.cloned.1.call-start = ((), (), s32[]{:S(2)}) async-start(), calls=%async_computation.1 | async-start | bytes 1310720 | tf_op jit(solution)/shard_map/all_gather | solution.py:42
  7.3 172.5 %reduce-scatter.2.cloned.1.call-start = ((), (), s32[]{:S(2)}) async-start(), calls=%async_computation.2 | async-start | bytes 1310720 | tf_op jit(solution)/shard_map/reduce_scatter | solution.py:148
  31.7 37.7 %copy-start.1 = (bf16[256,2048]{1,0:T(8,128)(2,1)S(1)}, bf16[256,2048]{1,0:T(8,128)(2,1)}, u32[]{:S(2)}) copy-start(bf16[256,2048]{1,0:T(8,128)(2,1)} %all-gather.2.cloned.1.call-done) | copy-start | bytes 3145732
  69.4 32.8 %copy-start.5 = (bf16[2048,256]{1,0:T(8,128)(2,1)S(1)}, bf16[2048,256]{1,0:T(8,128)(2,1)}, u32[]{:S(2)}) copy-start(bf16[2048,256]{1,0:T(8,128)(2,1)} %param.23) | copy-start | bytes 3145732
  102.9 13.8 %copy-start.4 = (f32[2]{0:T(128)S(1)}, f32[2]{0:T(128)}, u32[]{:S(2)}) copy-start(f32[2]{0:T(128)} %param.30) | copy-start | bytes 28
  102.9 14.2 %copy-start.2 = (f32[128]{0:T(128)S(1)}, f32[128]{0:T(128)}, u32[]{:S(2)}) copy-start(f32[128]{0:T(128)} %param.31) | copy-start | bytes 1540
  116.7 2.2 %copy-start.7 = (bf16[2048,128]{1,0:T(8,128)(2,1)S(1)}, bf16[2048,128]{1,0:T(8,128)(2,1)}, u32[]{:S(2)}) copy-start(bf16[2048,128]{1,0:T(8,128)(2,1)} %param.21) | copy-start | bytes 1572868
  117.4 8.5 %copy-start.6 = (bf16[2048,256]{1,0:T(8,128)(2,1)S(1)}, bf16[2048,256]{1,0:T(8,128)(2,1)}, u32[]{:S(2)}) copy-start(bf16[2048,256]{1,0:T(8,128)(2,1)} %param.27) | copy-start | bytes 3145732
  119.4 7.8 %collective-permute-start = (bf16[30,128]{1,0:T(8,128)(2,1)S(1)}, bf16[30,128]{1,0:T(8,128)(2,1)S(1)}, u32[]{:S(2)}, u32[]{:S(2)}) collective-permute-start(bf16[30,128]{1,0:T(8,128)(2,1)S(1)} %slice.274), channel_id=1, source_target_pairs={{0,4},{4,8},{8,12},{12,16},{16,20},{20,24},{24,28},{1,5},{5,9},{9,... | collective-permute-start | bytes 23048 | tf_op jit(solution)/shard_map/ppermute | solution.py:20
  127.3 6.4 %copy-start.3 = (f32[128]{0:T(128)S(1)}, f32[128]{0:T(128)}, u32[]{:S(2)}) copy-start(f32[128]{0:T(128)} %param.29) | copy-start | bytes 1540
Sparse Core Ops, SparseCore 0:
  8.9 19.4 all-gather.1
  137.6 42.1 reduce-scatter.1
where the time goes:
time: 187 us
  blocking collectives  70.6 us (38%)
  waiting for transfers between devices  62.3 us (33%)
  between operations  14.2 us (8%)
  matrix products  12 us (6%)
  local copies, waits for them, and re-layouts  10.2 us (5%)
  starting transfers between devices  6.53 us (3%)
  loops' own time  5.83 us (3%)
  other arithmetic  4.96 us (3%)
    reduce_scatter x1, waiting for transfers between devices, local(): lax.psum_scatter((jnp.dot(y_conv, out_conv, preferred_element_type=jnp.fl...  42.3 us
    all_gather x1, blocking collectives, local(): key_piece = lax.all_gather(key, 'sp', axis=0, tiled=True)  33.5 us
    all_gather x1, blocking collectives, local(): value_piece = lax.all_gather(value, 'sp', axis=0, tiled=True)  31.3 us
    all_gather x1, waiting for transfers between devices, local(): lax.all_gather(tokens, 'tp', axis=1, tiled=True).astype(jnp.float32)  18.6 us
    dot_general x6, matrix products, local(): jnp.dot(scaled, weight, preferred_element_type=jnp.float32)  6.52 us
    ppermute x1, starting transfers between devices, shifted(): return lax.ppermute(x, axis, pairs)  6.49 us
    psum x1, blocking collectives, local(): total_sq = lax.psum(jnp.sum(conv * conv, axis=1), 'tp')  5.8 us
    another operation x1, loops' own time, local(): lax.scan(visit, start_attn, (stacked_keys, stacked_values, firsts))  5.67 us
  transfers between devices with their start and end apart: 3, of which 3 were waited for; matrix products, arithmetic and copies ran while one was open for 1% of the time, Pallas kernels for 0%

commit v1 on v0

--- a/solution.py
+++ b/solution.py
@@ -78,7 +78,12 @@
             for rows_of, unused_pos in query_groups
         )
     )
-    key_piece = lax.all_gather(key, "sp", axis=0, tiled=True)
+    ring = [key]
+    for hop in range(7):
+        ring.append(lax.ppermute(ring[-1], "sp", [(dev, (dev + 1) % 8) for dev in range(8)]))
+    key_piece = jnp.roll(
+        jnp.concatenate(ring[::-1], axis=0), (lax.axis_index("sp") + 1) * ring[0].shape[0], axis=0
+    )
     value_piece = lax.all_gather(value, "sp", axis=0, tiled=True)
     shards = key_piece.shape[0] // tok_rows
     stacked_keys = key_piece.reshape(shards, tok_rows, kv_local, 2, QK)

time: 187 us -> 168 us (0.90)
  blocking collectives: 70.6 us -> 37.2 us
  waiting for transfers between devices: 62.3 us -> 76.8 us
  local copies, waits for them, and re-layouts: 10.2 us -> 8.16 us
    all_gather x1 -> x0, blocking collectives: 33.5 us -> none  [local(): key_piece = lax.all_gather(key, 'sp', axis=0, tiled=True)]
    ppermute x0 -> x7, waiting for transfers between devices: none -> 22.2 us  [local(): lax.ppermute(ring[-1], 'sp', [(dev, (dev + 1) % 8) for dev in range(8)])]
    reduce_scatter x1, waiting for transfers between devices: 42.3 us -> 35.4 us  [local(): lax.psum_scatter((jnp.dot(y_conv, out_conv, preferred_element_type=jnp.fl...]
    ppermute x0 -> x7, starting transfers between devices: none -> 4.76 us  [local(): lax.ppermute(ring[-1], 'sp', [(dev, (dev + 1) % 8) for dev in range(8)])]
    ppermute x1, starting transfers between devices: 6.49 us -> 3.38 us  [shifted(): return lax.ppermute(x, axis, pairs)]
    reshape x1, local copies, waits for them, and re-layouts: 2.45 us -> 0.4 us  [local(): stacked_keys = key_piece.reshape(shards, tok_rows, kv_local, 2, QK)]
  transfers between devices with their start and end apart: 3 -> 10, of which waited for: 3 -> 8; matrix products, arithmetic and copies ran while one was open for 1% -> 5% of each run, Pallas kernels for 0% -> 0%
where the time goes in v1:
time: 168 us; the launch traced here: 167 us
  waiting for transfers between devices  76.8 us (46%)
  blocking collectives  37.2 us (22%)
  between operations  14.3 us (9%)
  matrix products  11.5 us (7%)
  starting transfers between devices  8.18 us (5%)
  local copies, waits for them, and re-layouts  8.16 us (5%)
  loops' own time  5.94 us (4%)
  other arithmetic  5.04 us (3%)
    reduce_scatter x1, waiting for transfers between devices, local(): lax.psum_scatter((jnp.dot(y_conv, out_conv, preferred_element_type=jnp.fl...  35.4 us
    all_gather x1, blocking collectives, local(): value_piece = lax.all_gather(value, 'sp', axis=0, tiled=True)  31.4 us
    ppermute x7, waiting for transfers between devices, local(): lax.ppermute(ring[-1], 'sp', [(dev, (dev + 1) % 8) for dev in range(8)])  22.2 us
    all_gather x1, waiting for transfers between devices, local(): lax.all_gather(tokens, 'tp', axis=1, tiled=True).astype(jnp.float32)  18.5 us
    dot_general x6, matrix products, local(): jnp.dot(scaled, weight, preferred_element_type=jnp.float32)  5.87 us
    psum x1, blocking collectives, local(): total_sq = lax.psum(jnp.sum(conv * conv, axis=1), 'tp')  5.85 us
    another operation x1, loops' own time, local(): lax.scan(visit, start_attn, (stacked_keys, stacked_values, firsts))  5.78 us
    dynamic_slice x8, local copies, waits for them, and re-layouts, local(): lax.scan(visit, start_attn, (stacked_keys, stacked_values, firsts))  5.35 us
  transfers between devices with their start and end apart: 10, of which 8 were waited for; matrix products, arithmetic and copies ran while one was open for 5% of the time, Pallas kernels for 0%

profile of v1, /device:TPU:0, one launch (start us, length us, event | category | flops | bytes accessed | tf_op | source)
XLA Modules:
  0.0 167.2 jit_solution(10132876171140507593)
XLA Ops:
  6.5 0.7 all-gather.2.cloned.1.call-update
  7.3 0.7 convert_element_type.71
  8.5 0.7 convert_element_type.79
  9.8 18.5 %all-gather.2.cloned.1.call-done = bf16[256,2048]{1,0:T(8,128)(2,1)} async-done(((bf16[256,512]{1,0:T(8,128)(2,1)}), bf16[256,2048]{1,0:T(8,128)(2,1)}) %all-gather.2.cloned.1.call-update) | async-done | bytes 1048592 | tf_op jit(solution)/shard_map/all_gather | solution.py:42
  28.4 1.6 fusion.19
  30.0 1.8 %fusion.35 = bf16[256,128]{1,0:T(8,128)(2,1)S(1)} fusion(bf16[2048,128]{1,0:T(8,128)(2,1)} %param.24, bf16[256,2048]{1,0:T(8,128)(2,1)} %all-gather.2.cloned.1.call-done, f32[2048]{0:T(1024)S(1)} %convert_element_type.71, f32[256]{0:T(256)S(1)} %add_rsqrt_fusion.2), kind=kOutput, calls=%fused_computation.53 | convolution fusion | flops 135856128 | bytes 1647616 | tf_op jit(solution)/shard_map/dot_general | solution.py:46
  31.8 1.5 collective-permute-start.1
  34.3 3.4 %collective-permute-start = (bf16[30,128]{1,0:T(8,128)(2,1)S(1)}, bf16[30,128]{1,0:T(8,128)(2,1)S(1)}, u32[]{:S(2)}, u32[]{:S(2)}) collective-permute-start(bf16[30,128]{1,0:T(8,128)(2,1)S(1)} %slice.274), channel_id=1, source_target_pairs={{0,4},{4,8},{8,12},{12,16},{16,20},{20,24},{24,28},{1,5},{5,9},{9,... | collective-permute-start | bytes 23048 | tf_op jit(solution)/shard_map/ppermute | solution.py:20
  38.9 0.9 collective-permute-start.2
  40.2 5.6 %collective-permute-done.2 = bf16[256,128]{1,0:T(8,128)(2,1)S(1)} collective-permute-done((bf16[256,128]{1,0:T(8,128)(2,1)S(1)}, bf16[256,128]{1,0:T(8,128)(2,1)S(1)}, u32[]{:S(2)}, u32[]{:S(2)}) %collective-permute-start.2) | collective-permute-done | bytes 65568 | tf_op jit(solution)/shard_map/ppermute | solution.py:83
  45.8 31.4 %all_gather.7 = bf16[2048,128]{1,0:T(8,128)(2,1)S(1)} all-gather(bf16[256,128]{1,0:T(8,128)(2,1)S(1)} %fusion.36), channel_id=1, replica_groups=mesh['sp'=8,'tp'=4] {'sp'}, dimensions={0}, use_global_device_ids=true | all-gather | bytes 589824 | tf_op jit(solution)/shard_map/all_gather | solution.py:87
  77.2 2.3 %collective-permute-start.4 = (bf16[256,128]{1,0:T(8,128)(2,1)S(1)}, bf16[256,128]{1,0:T(8,128)(2,1)S(1)}, u32[]{:S(2)}, u32[]{:S(2)}) collective-permute-start(bf16[256,128]{1,0:T(8,128)(2,1)S(1)} %collective-permute-done.3), channel_id=1, source_target_pairs={{0,4},{4,8},{8,12},{12,16},{16,20},{20,24},{24,28},{28,0},{1,5},{5... | collective-permute-start | bytes 196616 | tf_op jit(solution)/shard_map/ppermute | solution.py:83
  79.5 4.8 %collective-permute-done.4 = bf16[256,128]{1,0:T(8,128)(2,1)S(1)} collective-permute-done((bf16[256,128]{1,0:T(8,128)(2,1)S(1)}, bf16[256,128]{1,0:T(8,128)(2,1)S(1)}, u32[]{:S(2)}, u32[]{:S(2)}) %collective-permute-start.4) | collective-permute-done | bytes 65568 | tf_op jit(solution)/shard_map/ppermute | solution.py:83
  84.9 5.8 %psum.7 = f32[256]{0:T(256)S(1)} all-reduce(f32[256]{0:T(256)S(1)} %get-tuple-element.287), channel_id=1, replica_groups=mesh['sp'=8,'tp'=4] {'tp'}, use_global_device_ids=true, to_apply=%region_2.3 | all-reduce | flops 256 | bytes 2048 | tf_op jit(solution)/shard_map/psum | solution.py:150
  91.3 7.0 %collective-permute-done.6 = bf16[256,128]{1,0:T(8,128)(2,1)S(1)} collective-permute-done((bf16[256,128]{1,0:T(8,128)(2,1)S(1)}, bf16[256,128]{1,0:T(8,128)(2,1)S(1)}, u32[]{:S(2)}, u32[]{:S(2)}) %collective-permute-start.6) | collective-permute-done | bytes 65568 | tf_op jit(solution)/shard_map/ppermute | solution.py:83
  98.3 3.3 %fusion.83 = f32[256,2048]{1,0:T(8,128)} fusion(bf16[128,2048]{1,0:T(8,128)(2,1)} %param.32, bf16[2048,128]{1,0:T(8,128)(2,1)} %param.26, bf16[256,2048]{1,0:T(8,128)(2,1)S(1)} %copy-done.2, f32[2048]{0:T(1024)S(1)} %convert_element_type.71, f32[256,128]{1,0:T(8,128)S(1)} %get-tuple-element.288, f32[128]{0:T(128)S(1)} %copy-done.3, ...), kind=kOutput, calls=%fused_computation.126 | convolution fusion | flops 270499840 | bytes 4336128 | tf_op jit(solution)/shard_map/dot_general | solution.py:155
  101.6 3.6 %collective-permute-done.7 = bf16[256,128]{1,0:T(8,128)(2,1)S(1)} collective-permute-done((bf16[256,128]{1,0:T(8,128)(2,1)S(1)}, bf16[256,128]{1,0:T(8,128)(2,1)S(1)}, u32[]{:S(2)}, u32[]{:S(2)}) %collective-permute-start.7) | collective-permute-done | bytes 65568 | tf_op jit(solution)/shard_map/ppermute | solution.py:83
  106.7 13.2 %while.17 = (s32[]{:T(128)}, f32[1,2,2,256]{3,1,2,0:T(2,128)S(1)}, f32[1,2,2,256]{3,1,2,0:T(2,128)S(1)}, f32[1,2,2,256,128]{4,3,2,1,0:T(8,128)S(1)}, s32[8]{0:T(...) while((s32[]{:T(128)}, f32[1,2,2,256]{3,1,2,0:T(2,128)S(1)}, ...), condition=%wide.region_8.9_spmd.clone, body=%wide.region_3.8_spmd.clone.sunk | while | flops 102567424 | bytes 4664615 | solution.py:131
  108.1 2.0 %conditional.3 = ((f32[1,2,2,256]{3,1,2,0:T(2,128)S(1)}, f32[1,2,2,256]{3,1,2,0:T(2,128)S(1)}, f32[1,2,2,256,128]{4,3,2,1,0:T(8,128)S(1)})) conditional(s32[]{:T(128)} %convert_element_type.190, (f32[1,2,2,256]{3,1,2,0:T(2,128)S(1)}, f32[1,2,2,256]{3,1,2,0:T(2,128)S(1)}, f32[1,2,2,256,128]{4,3,2,1,0:T(8,128)S(1)}) %tuple.82, (s32[]{:T(128)}, ...), branch_computations={%region_4.4_spmd, %region_5.7_spmd} | conditional | flops 102567424 | bytes 4663344 | solution.py:128
  108.1 0.7 broadcast_add_fusion
  120.5 0.8 copy.30
  121.3 2.2 %fusion.47 = bf16[256,256]{0,1:T(8,128)(2,1)S(1)} fusion(f32[256,1,2,128]{0,3,2,1:T(8,128)} %copy.30, bf16[2048,256]{1,0:T(8,128)(2,1)} %param.27, bf16[256,2048]{1,0:T(8,128)(2,1)} %all-gather.2.cloned.1.call-done, f32[2048]{0:T(1024)S(1)} %convert_element_type.71, f32[256]{0:T(256)S(1)} %add_rsqrt_fusion.2), kind=kOutput, calls=%fused_computation.60 | convolution fusion | flops 270598144 | bytes 2499584 | tf_op jit(solution)/shard_map/dot_general | solution.py:46
  123.5 1.4 fusion.17
  125.0 35.4 %reduce-scatter.2.cloned.1.call-done = bf16[64,2048]{1,0:T(8,128)(2,1)} async-done(((bf16[256,2048]{1,0:T(8,128)(2,1)}), bf16[64,2048]{1,0:T(8,128)(2,1)}) %reduce-scatter.2.cloned.1.call-update) | async-done | bytes 262160 | tf_op jit(solution)/shard_map/reduce_scatter | solution.py:153
  (103 shorter events, 12.8 us)
Async XLA Ops:
  6.5 116.9 %copy-start = (bf16[256,2048]{1,0:T(8,128)(2,1)S(1)}, bf16[256,2048]{1,0:T(8,128)(2,1)}, u32[]{:S(2)}) copy-start(bf16[256,2048]{1,0:T(8,128)(2,1)} %param.33) | copy-start | bytes 3145732
  6.5 26.8 %copy-start.7 = (bf16[2048,128]{1,0:T(8,128)(2,1)S(1)}, bf16[2048,128]{1,0:T(8,128)(2,1)}, u32[]{:S(2)}) copy-start(bf16[2048,128]{1,0:T(8,128)(2,1)} %param.22) | copy-start | bytes 1572868
  6.5 21.8 %all-gather.2.cloned.1.call-start = ((), (), s32[]{:S(2)}) async-start(), calls=%async_computation.1 | async-start | bytes 1310720 | tf_op jit(solution)/shard_map/all_gather | solution.py:42
  7.3 153.1 %reduce-scatter.2.cloned.1.call-start = ((), (), s32[]{:S(2)}) async-start(), calls=%async_computation.2 | async-start | bytes 1310720 | tf_op jit(solution)/shard_map/reduce_scatter | solution.py:153
  28.4 5.0 %copy-start.2 = (bf16[256,2048]{1,0:T(8,128)(2,1)S(1)}, bf16[256,2048]{1,0:T(8,128)(2,1)}, u32[]{:S(2)}) copy-start(bf16[256,2048]{1,0:T(8,128)(2,1)} %all-gather.2.cloned.1.call-done) | copy-start | bytes 3145732
  30.0 3.8 %copy-start.8 = (bf16[2048,128]{1,0:T(8,128)(2,1)S(1)}, bf16[2048,128]{1,0:T(8,128)(2,1)}, u32[]{:S(2)}) copy-start(bf16[2048,128]{1,0:T(8,128)(2,1)} %param.21) | copy-start | bytes 1572868
  31.8 5.8 %copy-start.6 = (bf16[2048,256]{1,0:T(8,128)(2,1)S(1)}, bf16[2048,256]{1,0:T(8,128)(2,1)}, u32[]{:S(2)}) copy-start(bf16[2048,256]{1,0:T(8,128)(2,1)} %param.23) | copy-start | bytes 3145732
  31.8 7.0 %collective-permute-start.1 = (bf16[256,128]{1,0:T(8,128)(2,1)S(1)}, bf16[256,128]{1,0:T(8,128)(2,1)S(1)}, u32[]{:S(2)}, u32[]{:S(2)}) collective-permute-start(bf16[256,128]{1,0:T(8,128)(2,1)S(1)} %fusion.35), channel_id=1, source_target_pairs={{0,4},{4,8},{8,12},{12,16},{16,20},{20,24},{24,28},{28,0},{1,5},{5... | collective-permute-start | bytes 196616 | tf_op jit(solution)/shard_map/ppermute | solution.py:83
  33.8 6.0 %copy-start.9 = (bf16[2048,128]{1,0:T(8,128)(2,1)S(1)}, bf16[2048,128]{1,0:T(8,128)(2,1)}, u32[]{:S(2)}) copy-start(bf16[2048,128]{1,0:T(8,128)(2,1)} %param.25) | copy-start | bytes 1572868
  34.3 45.3 %collective-permute-start = (bf16[30,128]{1,0:T(8,128)(2,1)S(1)}, bf16[30,128]{1,0:T(8,128)(2,1)S(1)}, u32[]{:S(2)}, u32[]{:S(2)}) collective-permute-start(bf16[30,128]{1,0:T(8,128)(2,1)S(1)} %slice.274), channel_id=1, source_target_pairs={{0,4},{4,8},{8,12},{12,16},{16,20},{20,24},{24,28},{1,5},{5,9},{9,... | collective-permute-start | bytes 23048 | tf_op jit(solution)/shard_map/ppermute | solution.py:20
  38.9 7.0 %collective-permute-start.2 = (bf16[256,128]{1,0:T(8,128)(2,1)S(1)}, bf16[256,128]{1,0:T(8,128)(2,1)S(1)}, u32[]{:S(2)}, u32[]{:S(2)}) collective-permute-start(bf16[256,128]{1,0:T(8,128)(2,1)S(1)} %collective-permute-done.1), channel_id=1, source_target_pairs={{0,4},{4,8},{8,12},{12,16},{16,20},{20,24},{24,28},{28,0},{1,5},{5... | collective-permute-start | bytes 196616 | tf_op jit(solution)/shard_map/ppermute | solution.py:83
  45.8 31.4 %collective-permute-start.3 = (bf16[256,128]{1,0:T(8,128)(2,1)S(1)}, bf16[256,128]{1,0:T(8,128)(2,1)S(1)}, u32[]{:S(2)}, u32[]{:S(2)}) collective-permute-start(bf16[256,128]{1,0:T(8,128)(2,1)S(1)} %collective-permute-done.2), channel_id=1, source_target_pairs={{0,4},{4,8},{8,12},{12,16},{16,20},{20,24},{24,28},{28,0},{1,5},{5... | collective-permute-start | bytes 196616 | tf_op jit(solution)/shard_map/ppermute | solution.py:83
  77.2 7.1 %collective-permute-start.4 = (bf16[256,128]{1,0:T(8,128)(2,1)S(1)}, bf16[256,128]{1,0:T(8,128)(2,1)S(1)}, u32[]{:S(2)}, u32[]{:S(2)}) collective-permute-start(bf16[256,128]{1,0:T(8,128)(2,1)S(1)} %collective-permute-done.3), channel_id=1, source_target_pairs={{0,4},{4,8},{8,12},{12,16},{16,20},{20,24},{24,28},{28,0},{1,5},{5... | collective-permute-start | bytes 196616 | tf_op jit(solution)/shard_map/ppermute | solution.py:83
  84.4 7.0 %collective-permute-start.5 = (bf16[256,128]{1,0:T(8,128)(2,1)S(1)}, bf16[256,128]{1,0:T(8,128)(2,1)S(1)}, u32[]{:S(2)}, u32[]{:S(2)}) collective-permute-start(bf16[256,128]{1,0:T(8,128)(2,1)S(1)} %collective-permute-done.4), channel_id=1, source_target_pairs={{0,4},{4,8},{8,12},{12,16},{16,20},{20,24},{24,28},{28,0},{1,5},{5... | collective-permute-start | bytes 196616 | tf_op jit(solution)/shard_map/ppermute | solution.py:83
  84.4 13.9 %copy-start.3 = (f32[128]{0:T(128)S(1)}, f32[128]{0:T(128)}, u32[]{:S(2)}) copy-start(f32[128]{0:T(128)} %param.29) | copy-start | bytes 1540
  91.3 7.0 %collective-permute-start.6 = (bf16[256,128]{1,0:T(8,128)(2,1)S(1)}, bf16[256,128]{1,0:T(8,128)(2,1)S(1)}, u32[]{:S(2)}, u32[]{:S(2)}) collective-permute-start(bf16[256,128]{1,0:T(8,128)(2,1)S(1)} %collective-permute-done.5), channel_id=1, source_target_pairs={{0,4},{4,8},{8,12},{12,16},{16,20},{20,24},{24,28},{28,0},{1,5},{5... | collective-permute-start | bytes 196616 | tf_op jit(solution)/shard_map/ppermute | solution.py:83
  98.3 7.0 %collective-permute-start.7 = (bf16[256,128]{1,0:T(8,128)(2,1)S(1)}, bf16[256,128]{1,0:T(8,128)(2,1)S(1)}, u32[]{:S(2)}, u32[]{:S(2)}) collective-permute-start(bf16[256,128]{1,0:T(8,128)(2,1)S(1)} %collective-permute-done.6), channel_id=1, source_target_pairs={{0,4},{4,8},{8,12},{12,16},{16,20},{20,24},{24,28},{28,0},{1,5},{5... | collective-permute-start | bytes 196616 | tf_op jit(solution)/shard_map/ppermute | solution.py:83
  106.7 13.2 %copy-start.5 = (f32[2]{0:T(128)S(1)}, f32[2]{0:T(128)}, u32[]{:S(2)}) copy-start(f32[2]{0:T(128)} %param.30) | copy-start | bytes 28
  106.7 13.6 %copy-start.4 = (f32[128]{0:T(128)S(1)}, f32[128]{0:T(128)}, u32[]{:S(2)}) copy-start(f32[128]{0:T(128)} %param.31) | copy-start | bytes 1540
  120.5 3.0 %copy-start.1 = (f32[256,2048]{1,0:T(8,128)S(1)}, f32[256,2048]{1,0:T(8,128)}, u32[]{:S(2)}) copy-start(f32[256,2048]{1,0:T(8,128)} %fusion.83) | copy-start | bytes 6291460
Sparse Core Ops, SparseCore 0:
  8.9 19.4 all-gather.1
  125.1 35.2 reduce-scatter.1
